TPU v7x, 32 devices: a whole 2x2x4 slice. The times are simulated.
32 devices in a mesh: grp: 2 (over y), sp: 4 (over z), tp: 4 (over x, core).
Axes of the slice: x: 2, y: 2, z: 4, core: 2. Of those that a mesh axis runs over, the one named last changes fastest.
Arguments:
- resid: bfloat16 [5120, 2048], P(('grp', 'sp'), 'tp'), parts along dimension 0, may hold values from -6 to 6
- queries: bfloat16 [5120, 2048], P(('grp', 'sp'), 'tp'), parts along dimension 0, may hold values from -150 to 150
- keys_values: bfloat16 [5120, 8, 128], P(('grp', 'sp'), 'tp'), parts along dimension 0, may hold values from -4.5 to 4.5
- sink: float32 [32], P('tp'), may hold values from 3 to 7
- out_weight: bfloat16 [2048, 2048], P('tp'), may hold values from -2.390625 to 2.390625
- norm_gain: float32 [2048], replicated, may hold values from 0.1 to 1.9
- gate_weight: bfloat16 [2048, 5632], P('sp', 'tp'), may hold values from -0.125 to 0.125
- up_weight: bfloat16 [2048, 5632], P('sp', 'tp'), may hold values from -0.125 to 0.125
- down_weight: bfloat16 [5632, 2048], P('tp', 'sp'), may hold values from -0.078125 to 0.078125
Outputs:
- mixed: bfloat16 [5120, 2048], P(('grp', 'sp'), 'tp'), parts along dimension 0
There are 2 independent parts, one for each index of `grp`. A program takes and returns all parts, laid end to end along the dimension named above; an argument that names none is the same for every part. Nothing has to cross between parts.
All inputs are finite; a program needn't handle non-finite values.
Results may differ from a plain program's by a relative error of at most 0.008.
Values may be sent and summed in bfloat16 or wider, within the bound.
A program may use at most 128 MiB of HBM per device.

v0:
```python
import jax
import jax.numpy as jnp
from jax import lax
from jax.sharding import PartitionSpec as P

HEAD_DIM = 64
WINDOW = 128
GRID_W = 64


def with_halo(cells, sides, width):
    for axis, dim in sides:
        count = lax.axis_size(axis)
        ends = count - 1
        head = lax.slice_in_dim(cells, 0, width, axis=dim)
        tail = lax.slice_in_dim(cells, cells.shape[dim] - width, cells.shape[dim], axis=dim)
        cells = jnp.concatenate(
            [
                lax.ppermute(tail, axis, [(i, (i + 1) % count) for i in range(ends)]),
                cells,
                lax.ppermute(head, axis, [((i + 1) % count, i) for i in range(ends)]),
            ],
            axis=dim,
        )
    return cells


def rotate(values, positions):
    quarter = 16
    inverse = 10000.0 ** (-jnp.arange(quarter, dtype=jnp.float32) / quarter)

    def turn(part, place):
        angle = place.astype(jnp.float32)[:, None] * inverse[None, :]
        cosine = jnp.cos(angle)[:, None, :]
        sine = jnp.sin(angle)[:, None, :]
        first, second = (part[..., :quarter], part[..., quarter:])
        return jnp.concatenate(
            [first * cosine - second * sine, second * cosine + first * sine], axis=-1
        )

    grid_row = positions // GRID_W
    grid_col = positions % GRID_W
    return jnp.concatenate(
        [turn(values[..., :32], grid_row), turn(values[..., 32:], grid_col)], axis=-1
    )


def body(
    resid, queries, keys_values, sink, out_weight, norm_gain, gate_weight, up_weight, down_weight
):
    tok = queries.shape[0]
    heads_here = queries.shape[1] // HEAD_DIM
    kv_here = keys_values.shape[1]
    group = heads_here // kv_here
    cols = resid.shape[1]
    offset = lax.axis_index("sp") * tok
    total_tokens = tok * lax.axis_size("sp")
    positions = offset + jnp.arange(tok, dtype=jnp.int32)
    rotated_q = rotate(
        queries.astype(jnp.float32).reshape(tok, heads_here, HEAD_DIM), positions
    ).astype(jnp.bfloat16)
    rotated_k = rotate(keys_values[..., :HEAD_DIM].astype(jnp.float32), positions).astype(
        jnp.bfloat16
    )
    joined = jnp.concatenate([rotated_k, keys_values[..., HEAD_DIM:]], axis=-1)
    padded = with_halo(joined, (("sp", 0),), WINDOW)
    blocks = tok // WINDOW
    key_blocks = jnp.stack(
        [padded[index * WINDOW : index * WINDOW + 3 * WINDOW] for index in range(blocks)]
    )
    grouped = rotated_q.reshape(blocks, WINDOW, kv_here, group, HEAD_DIM)
    scores = jnp.einsum(
        "nqkgd,njkd->nkgqj", grouped, key_blocks[..., :HEAD_DIM], preferred_element_type=jnp.float32
    ) * HEAD_DIM ** (-0.5)
    block_start = offset + WINDOW * jnp.arange(blocks, dtype=jnp.int32)
    query_pos = block_start[:, None] + jnp.arange(WINDOW, dtype=jnp.int32)[None, :]
    key_pos = block_start[:, None] - WINDOW + jnp.arange(3 * WINDOW, dtype=jnp.int32)[None, :]
    valid = (
        (jnp.abs(query_pos[:, :, None] - key_pos[:, None, :]) <= WINDOW)
        & (key_pos[:, None, :] >= 0)
        & (key_pos[:, None, :] < total_tokens)
    )
    scores = jnp.where(valid[:, None, None], scores, jnp.float32(-1e30))
    sink_grid = sink.reshape(kv_here, group)[None, :, :, None]
    top = jnp.maximum(jnp.max(scores, axis=-1), sink_grid)
    expo = jnp.exp(scores - top[..., None])
    denom = jnp.sum(expo, axis=-1) + jnp.exp(sink_grid - top)
    probs = (expo / denom[..., None]).astype(jnp.bfloat16)
    attended = jnp.einsum(
        "nkgqj,njkd->nqkgd", probs, key_blocks[..., HEAD_DIM:], preferred_element_type=jnp.float32
    )
    attended = attended.astype(jnp.bfloat16).reshape(tok, heads_here * HEAD_DIM)
    attn_rows, resid_rows = (
        lax.all_to_all(attended, "tp", split_axis=0, concat_axis=1, tiled=True),
        lax.all_to_all(resid, "tp", split_axis=0, concat_axis=1, tiled=True),
    )
    whole_out = lax.all_gather(out_weight, "tp", axis=0, tiled=True)
    stream_part = (
        resid_rows.astype(jnp.float32)
        + jnp.dot(attn_rows, whole_out, preferred_element_type=jnp.float32)
    ).astype(jnp.bfloat16)
    stream = lax.all_gather(stream_part, "tp", axis=0, tiled=True)
    stream_cols = lax.dynamic_slice_in_dim(stream, lax.axis_index("tp") * cols, cols, 1)
    widened = stream.astype(jnp.float32)
    normed = (
        widened * lax.rsqrt(jnp.mean(widened * widened, axis=-1, keepdims=True) + 1e-06) * norm_gain
    ).astype(jnp.bfloat16)
    gate = jnp.dot(
        normed,
        lax.all_gather(gate_weight, "sp", axis=0, tiled=True),
        preferred_element_type=jnp.float32,
    )
    up = jnp.dot(
        normed,
        lax.all_gather(up_weight, "sp", axis=0, tiled=True),
        preferred_element_type=jnp.float32,
    )
    hidden = (jax.nn.silu(gate) * up).astype(jnp.bfloat16)
    terms = jnp.dot(
        hidden,
        lax.all_gather(down_weight, "sp", axis=1, tiled=True),
        preferred_element_type=jnp.float32,
    )
    summed = lax.psum_scatter(
        terms.astype(jnp.bfloat16), "tp", scatter_dimension=1, tiled=True
    ).astype(jnp.float32)
    return (stream_cols.astype(jnp.float32) + summed).astype(jnp.bfloat16)


def solution(mesh):
    return jax.shard_map(
        body,
        mesh=mesh,
        in_specs=(
            P(("grp", "sp"), "tp"),
            P(("grp", "sp"), "tp"),
            P(("grp", "sp"), "tp", None),
            P("tp"),
            P("tp", None),
            P(),
            P("sp", "tp"),
            P("sp", "tp"),
            P("tp", "sp"),
        ),
        out_specs=P(("grp", "sp"), "tp"),
        check_vma=False,
    )
```

profile of v0, /device:TPU:0, one launch (start us, length us, event | category | flops | bytes accessed | tf_op | source)
XLA Modules:
  0.0 493.6 jit_solution(14125125992527969314)
XLA Ops:
  6.5 0.7 all-gather.6.cloned.1.call-update
  7.3 1.7 fusion.49
  8.9 0.2 copy.43
  9.2 0.2 copy.44
  9.4 0.4 multiply_cosine_fusion.1
  9.9 5.0 %collective-permute-start = (bf16[128,2,128]{0,2,1:T(8,128)(2,1)S(1)}, bf16[128,2,128]{0,2,1:T(8,128)(2,1)S(1)}, u32[]{:S(2)}, u32[]{:S(2)}) collective-permute-start(bf16[128,2,128]{0,2,1:T(8,128)(2,1)S(1)} %get-tuple-element.12), channel_id=1, source_target_pairs={{0,4},{4,8},{8,12},{1,5},{5,9},{9,13},{2,6},{6,10},{10,14},{3,7},{... | collective-permute-start | bytes 196616 | tf_op jit(solution)/shard_map/ppermute | solution.py:19
  14.9 1.3 collective-permute-start.1
  16.2 3.5 all-to-all-start
  19.7 0.3 copy.32
  20.1 0.1 convert.39
  20.2 0.1 iota_add_fusion.1
  20.2 0.1 fusion.36
  20.3 0.1 iota_add_fusion
  20.4 0.2 subtract_convert_fusion.1
  20.6 1.2 fusion.11
  21.8 0.2 concatenate.29
  22.0 0.2 concatenate.30
  22.2 0.2 concatenate.31
  22.5 0.2 concatenate.32
  22.7 0.1 max.17
  23.0 1.3 fusion.1
  24.3 0.1 broadcast_maximum_fusion
  24.4 1.9 fusion
  26.3 0.1 exponential_add_fusion
  26.4 2.3 fusion.9
  28.7 1.6 copy.38
  30.3 1.6 all_to_all.26
  31.9 5.0 %all-to-all-done = bf16[4,160,512]{2,1,0:T(8,128)(2,1)S(1)} async-done(((bf16[4,160,512]{2,1,0:T(8,128)(2,1)}), bf16[4,160,512]{2,1,0:T(8,128)(2,1)S(1)}, u32[]{:S(2)}, u32[]{:S(2)}) %all-to-all-start) | async-done | bytes 655392 | tf_op jit(solution)/shard_map/all_to_all | solution.py:95
  36.9 3.5 all-to-all-start.1
  40.5 0.2 convert_bitcast_fusion
  40.6 0.1 copy.45
  40.8 17.3 %all-to-all-done.1 = bf16[4,160,512]{2,1,0:T(8,128)(2,1)S(1)} async-done(((bf16[4,160,512]{2,1,0:T(8,128)(2,1)}), bf16[4,160,512]{2,1,0:T(8,128)(2,1)S(1)}, u32[]{:S(2)}, u32[]{:S(2)}) %all-to-all-start.1) | async-done | bytes 655392 | tf_op jit(solution)/shard_map/all_to_all | solution.py:94
  58.0 0.1 copy.46
  58.1 25.6 %all-gather.6.cloned.1.call-done = bf16[2048,2048]{1,0:T(8,128)(2,1)} async-done(((bf16[512,2048]{1,0:T(8,128)(2,1)}), bf16[2048,2048]{1,0:T(8,128)(2,1)}) %all-gather.6.cloned.1.call-update) | async-done | bytes 8388624 | tf_op jit(solution)/shard_map/all_gather | solution.py:97
  83.7 5.7 %fusion.7 = bf16[160,2048]{1,0:T(8,128)(2,1)} fusion(f32[160,2048]{1,0:T(8,128)S(1)} %bitcast.70, bf16[160,2048]{1,0:T(8,128)(2,1)S(1)} %bitcast.71, bf16[2048,2048]{1,0:T(8,128)(2,1)} %all-gather.6.cloned.1.call-done), kind=kOutput, calls=%fused_computation.15 | convolution fusion | flops 1342832640 | bytes 11010048 | tf_op jit(solution)/shard_map/dot_general | solution.py:100
  89.5 0.7 all-gather.10.cloned.1.call-update
  90.2 0.5 all-gather.12.cloned.1.call-update
  90.8 0.5 all-gather.14.cloned.1.call-update
  91.3 0.2 reduce-scatter.2.cloned.1.call-start
  91.6 23.8 %all-gather.8.cloned.1.call-done = bf16[640,2048]{1,0:T(8,128)(2,1)} async-done(((bf16[160,2048]{1,0:T(8,128)(2,1)}), bf16[640,2048]{1,0:T(8,128)(2,1)}) %all-gather.8.cloned.1.call-update) | async-done | bytes 2621456 | tf_op jit(solution)/shard_map/all_gather | solution.py:102
  115.4 2.3 fusion.2
  117.8 106.0 %all-gather.10.cloned.1.call-done = bf16[2048,1408]{1,0:T(8,128)(2,1)} async-done(((bf16[512,1408]{1,0:T(8,128)(2,1)}), bf16[2048,1408]{1,0:T(8,128)(2,1)}) %all-gather.10.cloned.1.call-update) | async-done | bytes 5767184 | tf_op jit(solution)/shard_map/all_gather | solution.py:110
  223.7 9.5 %fusion.14 = f32[640,1408]{1,0:T(8,128)} fusion(bf16[2048,1408]{1,0:T(8,128)(2,1)} %all-gather.10.cloned.1.call-done, bf16[640,2048]{1,0:T(8,128)(2,1)} %all-gather.8.cloned.1.call-done, f32[2048]{0:T(1024)S(1)} %copy-done.2, f32[640]{0:T(1024)S(1)} %add_rsqrt_fusion), kind=kOutput, calls=%fused_computation.23 | convolution fusion | flops 3696230400 | bytes 12003840 | tf_op jit(solution)/shard_map/dot_general | solution.py:108
  233.2 96.9 %all-gather.12.cloned.1.call-done = bf16[2048,1408]{1,0:T(8,128)(2,1)} async-done(((bf16[512,1408]{1,0:T(8,128)(2,1)}), bf16[2048,1408]{1,0:T(8,128)(2,1)}) %all-gather.12.cloned.1.call-update) | async-done | bytes 5767184 | tf_op jit(solution)/shard_map/all_gather | solution.py:115
  330.1 106.4 %all-gather.14.cloned.1.call-done = bf16[1408,2048]{1,0:T(8,128)(2,1)} async-done(((bf16[1408,512]{1,0:T(8,128)(2,1)}), bf16[1408,2048]{1,0:T(8,128)(2,1)}) %all-gather.14.cloned.1.call-update) | async-done | bytes 5767184 | tf_op jit(solution)/shard_map/all_gather | solution.py:121
  436.5 15.3 %convolution_convert_fusion = bf16[640,2048]{1,0:T(8,128)(2,1)} fusion(bf16[1408,2048]{1,0:T(8,128)(2,1)} %all-gather.14.cloned.1.call-done, bf16[2048,1408]{1,0:T(8,128)(2,1)} %all-gather.12.cloned.1.call-done, f32[640,1408]{1,0:T(8,128)} %fusion.14, bf16[640,2048]{1,0:T(8,128)(2,1)S(1)} %copy-done, f32[2048]{0:T(1024)S(1)} %copy-done.2, ...), kind=kOutput, calls=%fused_computation.13 | convolution fusion | flops 7393935360 | bytes 20392448 | tf_op jit(solution)/shard_map/dot_general | solution.py:119
  451.9 32.8 %reduce-scatter.2.cloned.1.call-done = bf16[640,512]{1,0:T(8,128)(2,1)} async-done(((bf16[640,2048]{1,0:T(8,128)(2,1)}), bf16[640,512]{1,0:T(8,128)(2,1)}) %reduce-scatter.2.cloned.1.call-update) | async-done | bytes 655376 | tf_op jit(solution)/shard_map/reduce_scatter | solution.py:124
  484.7 2.1 add_convert_fusion
  (37 shorter events, 0.7 us)
Async XLA Ops:
  6.5 13.2 %copy-start.1 = (bf16[640,512]{1,0:T(8,128)(2,1)S(1)}, bf16[640,512]{1,0:T(8,128)(2,1)}, u32[]{:S(2)}) copy-start(bf16[640,512]{1,0:T(8,128)(2,1)} %param.10) | copy-start | bytes 1966084
  6.5 77.1 %all-gather.6.cloned.1.call-start = ((), (), s32[]{:S(2)}) async-start(), calls=%async_computation.3 | async-start | bytes 10485760 | tf_op jit(solution)/shard_map/all_gather | solution.py:97
  9.9 12.9 %collective-permute-start = (bf16[128,2,128]{0,2,1:T(8,128)(2,1)S(1)}, bf16[128,2,128]{0,2,1:T(8,128)(2,1)S(1)}, u32[]{:S(2)}, u32[]{:S(2)}) collective-permute-start(bf16[128,2,128]{0,2,1:T(8,128)(2,1)S(1)} %get-tuple-element.12), channel_id=1, source_target_pairs={{0,4},{4,8},{8,12},{1,5},{5,9},{9,13},{2,6},{6,10},{10,14},{3,7},{... | collective-permute-start | bytes 196616 | tf_op jit(solution)/shard_map/ppermute | solution.py:19
  14.9 8.1 %collective-permute-start.1 = (bf16[128,2,128]{0,2,1:T(8,128)(2,1)S(1)}, bf16[128,2,128]{0,2,1:T(8,128)(2,1)S(1)}, u32[]{:S(2)}, u32[]{:S(2)}) collective-permute-start(bf16[128,2,128]{0,2,1:T(8,128)(2,1)S(1)} %get-tuple-element.11), channel_id=1, source_target_pairs={{4,0},{8,4},{12,8},{5,1},{9,5},{13,9},{6,2},{10,6},{14,10},{7,3},{... | collective-permute-start | bytes 196616 | tf_op jit(solution)/shard_map/ppermute | solution.py:21
  16.2 20.7 %all-to-all-start = ((bf16[4,160,512]{2,1,0:T(8,128)(2,1)}), bf16[4,160,512]{2,1,0:T(8,128)(2,1)S(1)}, u32[]{:S(2)}, u32[]{:S(2)}) async-start(bf16[4,160,512]{2,1,0:T(8,128)(2,1)} %bitcast), calls=%async_computation | async-start | bytes 1310720 | tf_op jit(solution)/shard_map/all_to_all | solution.py:95
  20.0 2.7 copy-start.3
  36.9 21.1 %all-to-all-start.1 = ((bf16[4,160,512]{2,1,0:T(8,128)(2,1)}), bf16[4,160,512]{2,1,0:T(8,128)(2,1)S(1)}, u32[]{:S(2)}, u32[]{:S(2)}) async-start(bf16[4,160,512]{2,1,0:T(8,128)(2,1)} %all_to_all.26), calls=%async_computation.1 | async-start | bytes 1310720 | tf_op jit(solution)/shard_map/all_to_all | solution.py:94
  40.4 75.0 %all-gather.8.cloned.1.call-start = ((), (), s32[]{:S(2)}) async-start(), calls=%async_computation.4 | async-start | bytes 3276800 | tf_op jit(solution)/shard_map/all_gather | solution.py:102
  89.4 134.3 %copy-start.2 = (f32[2048]{0:T(1024)S(1)}, f32[2048]{0:T(1024)}, u32[]{:S(2)}) copy-start(f32[2048]{0:T(1024)} %param.14) | copy-start | bytes 24580
  89.4 134.3 %all-gather.10.cloned.1.call-start = ((), (), s32[]{:S(2)}) async-start(), calls=%async_computation.5 | async-start | bytes 7208960 | tf_op jit(solution)/shard_map/all_gather | solution.py:110
  90.2 239.9 %all-gather.12.cloned.1.call-start = ((), (), s32[]{:S(2)}) async-start(), calls=%async_computation.6 | async-start | bytes 7208960 | tf_op jit(solution)/shard_map/all_gather | solution.py:115
  90.8 345.8 %all-gather.14.cloned.1.call-start = ((), (), s32[]{:S(2)}) async-start(), calls=%async_computation.7 | async-start | bytes 7208960 | tf_op jit(solution)/shard_map/all_gather | solution.py:121
  91.3 393.3 %reduce-scatter.2.cloned.1.call-start = ((), (), s32[]{:S(2)}) async-start(), calls=%async_computation.8 | async-start | bytes 3276800 | tf_op jit(solution)/shard_map/reduce_scatter | solution.py:124
  117.7 318.8 %copy-start = (bf16[640,2048]{1,0:T(8,128)(2,1)S(1)}, bf16[640,2048]{1,0:T(8,128)(2,1)}, u32[]{:S(2)}) copy-start(bf16[640,2048]{1,0:T(8,128)(2,1)} %all-gather.8.cloned.1.call-done) | copy-start | bytes 7864324
Sparse Core Ops, SparseCore 0:
  8.9 74.7 all-gather.5
  89.6 25.8 all-gather.7
  117.0 106.6 all-gather.9
  225.1 104.9 all-gather.11
  331.5 104.9 all-gather.13
  452.0 32.6 reduce-scatter.1
where the time goes:
time: 494 us
  waiting for transfers between devices  416 us (84%)
  matrix products  34.2 us (7%)
  between operations  13.8 us (3%)
  starting transfers between devices  13.6 us (3%)
  other arithmetic  8.95 us (2%)
  local copies, waits for them, and re-layouts  6.91 us (1%)
    all_gather x1, waiting for transfers between devices, body(): lax.all_gather(down_weight, 'sp', axis=1, tiled=True)  106 us
    all_gather x1, waiting for transfers between devices, body(): lax.all_gather(gate_weight, 'sp', axis=0, tiled=True)  106 us
    all_gather x1, waiting for transfers between devices, body(): lax.all_gather(up_weight, 'sp', axis=0, tiled=True)  96.9 us
    reduce_scatter x1, waiting for transfers between devices, body(): lax.psum_scatter(terms.astype(jnp.bfloat16), 'tp', scatter_dimension=1, t...  32.8 us
    all_gather x1, waiting for transfers between devices, body(): whole_out = lax.all_gather(out_weight, 'tp', axis=0, tiled=True)  25.6 us
    all_gather x1, waiting for transfers between devices, body(): stream = lax.all_gather(stream_part, 'tp', axis=0, tiled=True)  23.8 us
    all_to_all x1, waiting for transfers between devices, body(): lax.all_to_all(attended, 'tp', split_axis=0, concat_axis=1, tiled=True)  17.3 us
    dot_general x1, matrix products, body(): jnp.dot(hidden, lax.all_gather(down_weight, 'sp', axis=1, tiled=True), pr...  15.3 us
  transfers between devices with their start and end apart: 10, of which 8 were waited for; matrix products, arithmetic and copies ran while one was open for 5% of the time, Pallas kernels for 0%

commit v1 on v0

--- a/solution.py
+++ b/solution.py
@@ -94,7 +94,12 @@
         lax.all_to_all(attended, "tp", split_axis=0, concat_axis=1, tiled=True),
         lax.all_to_all(resid, "tp", split_axis=0, concat_axis=1, tiled=True),
     )
-    whole_out = lax.all_gather(out_weight, "tp", axis=0, tiled=True)
+    ring = [out_weight]
+    for hop in range(3):
+        ring.append(lax.ppermute(ring[-1], "tp", [(dev, (dev + 1) % 4) for dev in range(4)]))
+    whole_out = jnp.roll(
+        jnp.concatenate(ring[::-1], axis=0), (lax.axis_index("tp") + 1) * ring[0].shape[0], axis=0
+    )
     stream_part = (
         resid_rows.astype(jnp.float32)
         + jnp.dot(attn_rows, whole_out, preferred_element_type=jnp.float32)

time: 494 us -> 514 us (1.040)
  local copies, waits for them, and re-layouts: 6.91 us -> 22 us
    ppermute x0 -> x3, waiting for transfers between devices: none -> 31.9 us  [body(): lax.ppermute(ring[-1], 'tp', [(dev, (dev + 1) % 4) for dev in range(4)])]
    all_gather x1 -> x0, waiting for transfers between devices: 25.6 us -> none  [body(): whole_out = lax.all_gather(out_weight, 'tp', axis=0, tiled=True)]
    all_gather x1, waiting for transfers between devices: 96.9 us -> 106 us  [body(): lax.all_gather(up_weight, 'sp', axis=0, tiled=True)]
    all_gather x1, waiting for transfers between devices: 106 us -> 97.1 us  [body(): lax.all_gather(down_weight, 'sp', axis=1, tiled=True)]
    unnamed x14 -> x17, local copies, waits for them, and re-layouts: 0.78 us -> 9.95 us
  transfers between devices with their start and end apart: 10 -> 12, of which waited for: 8 -> 8; matrix products, arithmetic and copies ran while one was open for 5% -> 7% of each run, Pallas kernels for 0% -> 0%
where the time goes in v1:
time: 514 us; the launch traced here: 513 us
  waiting for transfers between devices  419 us (82%)
  matrix products  33.4 us (6%)
  local copies, waits for them, and re-layouts  22 us (4%)
  starting transfers between devices  15 us (3%)
  between operations  13.5 us (3%)
  other arithmetic  10.8 us (2%)
    all_gather x1, waiting for transfers between devices, body(): lax.all_gather(up_weight, 'sp', axis=0, tiled=True)  106 us
    all_gather x1, waiting for transfers between devices, body(): lax.all_gather(gate_weight, 'sp', axis=0, tiled=True)  106 us
    all_gather x1, waiting for transfers between devices, body(): lax.all_gather(down_weight, 'sp', axis=1, tiled=True)  97.1 us
    reduce_scatter x1, waiting for transfers between devices, body(): lax.psum_scatter(terms.astype(jnp.bfloat16), 'tp', scatter_dimension=1, t...  32.8 us
    ppermute x3, waiting for transfers between devices, body(): lax.ppermute(ring[-1], 'tp', [(dev, (dev + 1) % 4) for dev in range(4)])  31.9 us
    all_gather x1, waiting for transfers between devices, body(): stream = lax.all_gather(stream_part, 'tp', axis=0, tiled=True)  26.9 us
    dot_general x1, matrix products, body(): jnp.dot(hidden, lax.all_gather(down_weight, 'sp', axis=1, tiled=True), pr...  16.1 us
    all_to_all x1, waiting for transfers between devices, body(): lax.all_to_all(attended, 'tp', split_axis=0, concat_axis=1, tiled=True)  15.8 us
  transfers between devices with their start and end apart: 12, of which 8 were waited for; matrix products, arithmetic and copies ran while one was open for 7% of the time, Pallas kernels for 0%

profile of v1, /device:TPU:0, one launch (start us, length us, event | category | flops | bytes accessed | tf_op | source)
XLA Modules:
  0.0 513.4 jit_solution(10297042893464521922)
XLA Ops:
  6.5 0.5 collective-permute-start.2
  7.0 1.7 fusion.57
  9.1 0.4 multiply_cosine_fusion.1
  9.6 0.7 fusion.56
  10.3 4.5 collective-permute-start
  14.8 1.3 collective-permute-start.1
  16.1 4.2 all-to-all-start
  20.4 15.9 %collective-permute-done.2 = bf16[512,2048]{1,0:T(8,128)(2,1)S(1)} collective-permute-done((bf16[512,2048]{1,0:T(8,128)(2,1)}, bf16[512,2048]{1,0:T(8,128)(2,1)S(1)}, u32[]{:S(2)}, u32[]{:S(2)}) %collective-permute-start.2) | collective-permute-done | bytes 2097184 | tf_op jit(solution)/shard_map/ppermute | solution.py:99
  36.5 1.4 copy.32
  38.0 0.8 subtract_convert_fusion.1
  38.8 1.2 fusion.18
  40.0 1.1 concatenate.35
  41.1 0.7 copy.33
  41.8 0.2 concatenate.36
  42.0 0.7 copy.34
  42.7 0.2 concatenate.37
  42.9 0.2 concatenate.38
  43.2 0.7 max.17
  44.1 2.3 fusion.3
  46.5 16.0 %collective-permute-done.3 = bf16[512,2048]{1,0:T(8,128)(2,1)} collective-permute-done((bf16[512,2048]{1,0:T(8,128)(2,1)S(1)}, bf16[512,2048]{1,0:T(8,128)(2,1)}, u32[]{:S(2)}, u32[]{:S(2)}) %collective-permute-start.3) | collective-permute-done | bytes 2097184 | tf_op jit(solution)/shard_map/ppermute | solution.py:99
  62.5 1.9 fusion.2
  64.5 3.1 fusion.16
  67.5 2.8 copy.38
  70.3 1.6 all_to_all.26
  71.9 4.2 all-to-all-start.1
  76.1 0.2 all-gather.5.cloned.1.call-start
  76.3 1.2 convert_bitcast_fusion
  77.7 15.8 %all-to-all-done.1 = bf16[4,160,512]{2,1,0:T(8,128)(2,1)} async-done(((bf16[4,160,512]{2,1,0:T(8,128)(2,1)}), bf16[4,160,512]{2,1,0:T(8,128)(2,1)}, u32[]{:S(2)}, u32[]{:S(2)}) %all-to-all-start.1) | async-done | bytes 655392 | tf_op jit(solution)/shard_map/all_to_all | solution.py:94
  93.5 1.1 copy.46
  94.7 1.8 constant_dynamic-update-slice_fusion.8
  96.5 2.0 constant_dynamic-update-slice_fusion.7
  98.5 0.2 constant_dynamic-update-slice_fusion.6
  98.9 1.8 constant_dynamic-update-slice_fusion.4
  100.7 1.8 constant_dynamic-update-slice_fusion.3
  102.6 0.2 constant_dynamic-update-slice_fusion.2
  103.0 2.5 fusion.12
  105.5 0.7 all-gather.7.cloned.1.call-update
  106.3 0.7 all-gather.11.cloned.1.call-update
  107.0 0.5 all-gather.9.cloned.1.call-update
  107.6 26.9 %all-gather.5.cloned.1.call-done = bf16[640,2048]{1,0:T(8,128)(2,1)} async-done(((bf16[160,2048]{1,0:T(8,128)(2,1)}), bf16[640,2048]{1,0:T(8,128)(2,1)}) %all-gather.5.cloned.1.call-update) | async-done | bytes 2621456 | tf_op jit(solution)/shard_map/all_gather | solution.py:107
  134.5 2.3 fusion.4
  136.8 106.0 %all-gather.7.cloned.1.call-done = bf16[2048,1408]{1,0:T(8,128)(2,1)} async-done(((bf16[512,1408]{1,0:T(8,128)(2,1)}), bf16[2048,1408]{1,0:T(8,128)(2,1)}) %all-gather.7.cloned.1.call-update) | async-done | bytes 5767184 | tf_op jit(solution)/shard_map/all_gather | solution.py:115
  242.7 9.5 %fusion.21 = f32[640,1408]{1,0:T(8,128)} fusion(bf16[2048,1408]{1,0:T(8,128)(2,1)} %all-gather.7.cloned.1.call-done, bf16[640,2048]{1,0:T(8,128)(2,1)} %all-gather.5.cloned.1.call-done, f32[2048]{0:T(1024)S(1)} %copy-done.1, f32[640]{0:T(1024)S(1)} %add_rsqrt_fusion), kind=kOutput, calls=%fused_computation.25 | convolution fusion | flops 3696230400 | bytes 12003840 | tf_op jit(solution)/shard_map/dot_general | solution.py:113
  252.2 97.1 %all-gather.11.cloned.1.call-done = bf16[1408,2048]{1,0:T(8,128)(2,1)} async-done(((bf16[1408,512]{1,0:T(8,128)(2,1)}), bf16[1408,2048]{1,0:T(8,128)(2,1)}) %all-gather.11.cloned.1.call-update) | async-done | bytes 5767184 | tf_op jit(solution)/shard_map/all_gather | solution.py:126
  349.3 106.4 %all-gather.9.cloned.1.call-done = bf16[2048,1408]{1,0:T(8,128)(2,1)} async-done(((bf16[512,1408]{1,0:T(8,128)(2,1)}), bf16[2048,1408]{1,0:T(8,128)(2,1)}) %all-gather.9.cloned.1.call-update) | async-done | bytes 5767184 | tf_op jit(solution)/shard_map/all_gather | solution.py:120
  455.7 16.1 %convolution_convert_fusion = bf16[640,2048]{1,0:T(8,128)(2,1)} fusion(bf16[1408,2048]{1,0:T(8,128)(2,1)} %all-gather.11.cloned.1.call-done, bf16[2048,1408]{1,0:T(8,128)(2,1)} %all-gather.9.cloned.1.call-done, f32[640,1408]{1,0:T(8,128)} %fusion.21, bf16[640,2048]{1,0:T(8,128)(2,1)} %all-gather.5.cloned.1.call-done, f32[2048]{0:T(1024)S(1)} %copy-done.1, ...), kind=kOutput, calls=%fused_computation.15 | convolution fusion | flops 7393935360 | bytes 20392448 | tf_op jit(solution)/shard_map/dot_general | solution.py:124
  471.8 32.8 %reduce-scatter.2.cloned.1.call-done = bf16[640,512]{1,0:T(8,128)(2,1)} async-done(((bf16[640,2048]{1,0:T(8,128)(2,1)}), bf16[640,512]{1,0:T(8,128)(2,1)}) %reduce-scatter.2.cloned.1.call-update) | async-done | bytes 655376 | tf_op jit(solution)/shard_map/reduce_scatter | solution.py:129
  504.6 2.3 add_convert_fusion
  (44 shorter events, 1.9 us)
Async XLA Ops:
  6.5 29.8 %collective-permute-start.2 = (bf16[512,2048]{1,0:T(8,128)(2,1)}, bf16[512,2048]{1,0:T(8,128)(2,1)S(1)}, u32[]{:S(2)}, u32[]{:S(2)}) collective-permute-start(bf16[512,2048]{1,0:T(8,128)(2,1)} %param.13), channel_id=1, source_target_pairs={{0,1},{1,2},{2,3},{3,0},{4,5},{5,6},{6,7},{7,4},{8,9},{9,10},{10,1... | collective-permute-start | bytes 6291464 | tf_op jit(solution)/shard_map/ppermute | solution.py:99
  10.3 33.6 %collective-permute-start = (bf16[128,2,128]{0,2,1:T(8,128)(2,1)}, bf16[128,2,128]{0,2,1:T(8,128)(2,1)S(1)}, u32[]{:S(2)}, u32[]{:S(2)}) collective-permute-start(bf16[128,2,128]{0,2,1:T(8,128)(2,1)} %get-tuple-element.12), channel_id=1, source_target_pairs={{0,4},{4,8},{8,12},{1,5},{5,9},{9,13},{2,6},{6,10},{10,14},{3,7},{... | collective-permute-start | bytes 196616 | tf_op jit(solution)/shard_map/ppermute | solution.py:19
  14.8 29.3 %collective-permute-start.1 = (bf16[128,2,128]{0,2,1:T(8,128)(2,1)}, bf16[128,2,128]{0,2,1:T(8,128)(2,1)S(1)}, u32[]{:S(2)}, u32[]{:S(2)}) collective-permute-start(bf16[128,2,128]{0,2,1:T(8,128)(2,1)} %get-tuple-element.11), channel_id=1, source_target_pairs={{4,0},{8,4},{12,8},{5,1},{9,5},{13,9},{6,2},{10,6},{14,10},{7,3},{... | collective-permute-start | bytes 196616 | tf_op jit(solution)/shard_map/ppermute | solution.py:21
  16.1 55.8 %all-to-all-start = ((bf16[4,160,512]{2,1,0:T(8,128)(2,1)}), bf16[4,160,512]{2,1,0:T(8,128)(2,1)}, u32[]{:S(2)}, u32[]{:S(2)}) async-start(bf16[4,160,512]{2,1,0:T(8,128)(2,1)} %bitcast.72), calls=%async_computation | async-start | bytes 1310720 | tf_op jit(solution)/shard_map/all_to_all | solution.py:95
  36.4 26.1 %collective-permute-start.3 = (bf16[512,2048]{1,0:T(8,128)(2,1)S(1)}, bf16[512,2048]{1,0:T(8,128)(2,1)}, u32[]{:S(2)}, u32[]{:S(2)}) collective-permute-start(bf16[512,2048]{1,0:T(8,128)(2,1)S(1)} %collective-permute-done.2), channel_id=1, source_target_pairs={{0,1},{1,2},{2,3},{3,0},{4,5},{5,6},{6,7},{7,4},{8,9},{9,10},{10,1... | collective-permute-start | bytes 6291464 | tf_op jit(solution)/shard_map/ppermute | solution.py:99
  62.5 32.2 %collective-permute-start.4 = (bf16[512,2048]{1,0:T(8,128)(2,1)}, bf16[512,2048]{1,0:T(8,128)(2,1)}, u32[]{:S(2)}, u32[]{:S(2)}) collective-permute-start(bf16[512,2048]{1,0:T(8,128)(2,1)} %collective-permute-done.3), channel_id=1, source_target_pairs={{0,1},{1,2},{2,3},{3,0},{4,5},{5,6},{6,7},{7,4},{8,9},{9,10},{10,1... | collective-permute-start | bytes 6291464 | tf_op jit(solution)/shard_map/ppermute | solution.py:99
  71.9 21.6 %all-to-all-start.1 = ((bf16[4,160,512]{2,1,0:T(8,128)(2,1)}), bf16[4,160,512]{2,1,0:T(8,128)(2,1)}, u32[]{:S(2)}, u32[]{:S(2)}) async-start(bf16[4,160,512]{2,1,0:T(8,128)(2,1)} %all_to_all.26), calls=%async_computation.1 | async-start | bytes 1310720 | tf_op jit(solution)/shard_map/all_to_all | solution.py:94
  76.1 58.4 %all-gather.5.cloned.1.call-start = ((), (), s32[]{:S(2)}) async-start(), calls=%async_computation.3 | async-start | bytes 3276800 | tf_op jit(solution)/shard_map/all_gather | solution.py:107
  96.5 2.2 copy-start
  105.5 137.3 %copy-start.1 = (f32[2048]{0:T(1024)S(1)}, f32[2048]{0:T(1024)}, u32[]{:S(2)}) copy-start(f32[2048]{0:T(1024)} %param.14) | copy-start | bytes 24580
  105.5 137.3 %all-gather.7.cloned.1.call-start = ((), (), s32[]{:S(2)}) async-start(), calls=%async_computation.4 | async-start | bytes 7208960 | tf_op jit(solution)/shard_map/all_gather | solution.py:115
  106.2 243.1 %all-gather.11.cloned.1.call-start = ((), (), s32[]{:S(2)}) async-start(), calls=%async_computation.6 | async-start | bytes 7208960 | tf_op jit(solution)/shard_map/all_gather | solution.py:126
  107.0 348.7 %all-gather.9.cloned.1.call-start = ((), (), s32[]{:S(2)}) async-start(), calls=%async_computation.5 | async-start | bytes 7208960 | tf_op jit(solution)/shard_map/all_gather | solution.py:120
  107.5 397.0 %reduce-scatter.2.cloned.1.call-start = ((), (), s32[]{:S(2)}) async-start(), calls=%async_computation.7 | async-start | bytes 3276800 | tf_op jit(solution)/shard_map/reduce_scatter | solution.py:129
Sparse Core Ops, SparseCore 0:
  105.6 28.8 all-gather.4
  136.0 106.6 all-gather.6
  244.3 104.9 all-gather.10
  350.7 104.9 all-gather.8
  471.9 32.6 reduce-scatter.1
